TPU v7x, 512 devices: a whole 4x8x8 slice. The times are simulated.
512 devices in a mesh: sp: 64 (over z, y), tp: 8 (over x, core).
Axes of the slice: x: 4, y: 8, z: 8, core: 2. Of those that a mesh axis runs over, the one named last changes fastest.
Arguments:
- residual: bfloat16 [8192, 2048], P('sp', 'tp'), may hold values from -24 to 24
- queries: bfloat16 [8192, 2048], P('sp', 'tp'), may hold values from -16 to 16
- key_proj: bfloat16 [8192, 512], P(('sp', 'tp')), may hold values from -8 to 8
- value_proj: bfloat16 [8192, 512], P(('sp', 'tp')), may hold values from -6 to 6
- diff_lambda: float32 [8], replicated, may hold values from 0.3 to 0.8
- head_gain: float32 [256], replicated, may hold values from 0.1 to 1.9
- out_weight: bfloat16 [2048, 2048], P(None, 'tp'), may hold values from -0.125 to 0.125
- norm_gain: float32 [2048], P('tp'), may hold values from 0.1 to 1.9
- up_weight: bfloat16 [2048, 8192], P('sp', 'tp'), may hold values from -0.125 to 0.125
- down_weight: bfloat16 [8192, 2048], P('tp', 'sp'), may hold values from -0.0625 to 0.0625
Outputs:
- layer_out: bfloat16 [8192, 2048], P('sp', 'tp')
All inputs are finite; a program needn't handle non-finite values.
Results may differ from a plain program's by a relative error of at most 0.012.
Values may be sent and summed in bfloat16 or wider, within the bound.
A program may use at most 64 MiB of HBM per device.

v0:
```python
import jax
import jax.numpy as jnp
from jax import lax
from jax.sharding import PartitionSpec as P

D = 2048
HEADS = 8
KV_HEADS = 2
HEAD_DIM = 128
VALUE_DIM = 256
epsilon = 1e-06


def turned_gather(arrays, axis, dims):
    turned = [jnp.moveaxis(a, dim, 0) for a, dim in zip(arrays, dims)]
    both = jnp.concatenate([t.reshape(len(t), -1) for t in turned], axis=1)
    whole, at, finished = (lax.all_gather(both, axis, axis=0, tiled=True), 0, [])
    for t, dim in zip(turned, dims):
        share = whole[:, at : at + t[0].size].reshape(-1, *t.shape[1:])
        finished.append(jnp.moveaxis(share, 0, dim))
        at += t[0].size
    return tuple(finished)


def from_everyone(shard, axis):
    copies = jnp.broadcast_to(shard, (lax.axis_size(axis), *shard.shape))
    return lax.all_to_all(copies, axis, split_axis=0, concat_axis=0, tiled=True)


def laid_out(parts, dim):
    dims = list(parts.shape[1:])
    dims[dim] *= parts.shape[0]
    return jnp.moveaxis(parts, 0, dim).reshape(dims)


def collect(shard, axis, dim):
    parts = from_everyone(shard, axis)
    return laid_out(parts, dim)


def sent_together(arrays, axis, dim, along):
    ends, at = ([], 0)
    for a in arrays[:-1]:
        at += a.shape[along]
        ends.append(at)
    both = jnp.concatenate(arrays, axis=along)
    return tuple(jnp.split(lax.all_gather(both, axis, axis=dim, tiled=True), ends, axis=along))


def side_by_side(arrays, axis, split_dim, concat_dim, along):
    columns = [a.reshape(*a.shape[:along], -1) for a in arrays]
    both = jnp.concatenate(columns, axis=along)
    whole, at, finished = (
        lax.all_to_all(both, axis, split_axis=split_dim, concat_axis=concat_dim, tiled=True),
        0,
        [],
    )
    for a, column in zip(arrays, columns):
        share = whole[..., at : at + column.shape[along]]
        finished.append(share.reshape(*share.shape[:along], *a.shape[along:]))
        at += column.shape[along]
    return tuple(finished)


def over_copies(shard, axis):
    everything = from_everyone(shard, axis)
    return jnp.sum(everything, axis=0)


def split_up(shard, dim, length):
    dims = shard.shape
    parts = shard.reshape(*dims[:dim], length, dims[dim] // length, *dims[dim + 1 :])
    return jnp.moveaxis(parts, dim, 0)


def sent_and_summed(shard, axis, dim):
    parts = split_up(shard, dim, lax.axis_size(axis))
    arrived = lax.all_to_all(parts, axis, split_axis=0, concat_axis=0, tiled=True)
    return arrived.sum(axis=0)


def head_norm(per_map, lambdas, gain):
    difference = per_map[:, 0] - lambdas[:, None, None] * per_map[:, 1]
    scaled = (
        difference
        * lax.rsqrt(jnp.mean(difference * difference, axis=-1, keepdims=True) + epsilon)
        * gain
    )
    return scaled.astype(jnp.bfloat16)


def on_device(
    residual,
    queries,
    key_proj,
    value_proj,
    diff_lambda,
    head_gain,
    out_weight,
    norm_gain,
    up_weight,
    down_weight,
):
    up_whole, down_whole = turned_gather((up_weight, down_weight), "sp", (0, 1))
    rows_here = residual.shape[0]
    per_group = HEADS // KV_HEADS
    scaling = HEAD_DIM ** (-0.5)
    all_queries = collect(queries, "tp", 1)
    query_grid = all_queries.reshape(rows_here, KV_HEADS, per_group, 2, HEAD_DIM)
    stat_shape = (KV_HEADS, per_group, 2, rows_here)
    maxima = jnp.full(stat_shape, -1e30, jnp.float32)
    key_piece, value_piece = sent_together((key_proj, value_proj), "sp", 0, 1)
    key_count = key_piece.shape[0]
    key_grid = key_piece.reshape(key_count, KV_HEADS, 2, HEAD_DIM)
    value_grid = value_piece.reshape(key_count, KV_HEADS, VALUE_DIM)
    scores = (
        jnp.einsum("qagcd,kacd->agcqk", query_grid, key_grid, preferred_element_type=jnp.float32)
        * scaling
    )
    highest = jnp.maximum(maxima, jnp.max(scores, axis=-1))
    weights = jnp.exp(scores - highest[..., None])
    totals = jnp.sum(weights, axis=-1)
    weighted = jnp.einsum(
        "agcqk,kae->agcqe",
        weights.astype(jnp.bfloat16),
        value_grid,
        preferred_element_type=jnp.float32,
    )
    maxima, totals, weighted = (highest, totals, weighted)
    maxima = maxima.reshape(HEADS, 2, rows_here)
    totals = totals.reshape(HEADS, 2, rows_here)
    weighted = weighted.reshape(HEADS, 2, rows_here, VALUE_DIM)
    tp_size = lax.axis_size("tp")
    local_heads = HEADS // tp_size
    got_max, got_tot, got_sum = side_by_side((maxima, totals, weighted), "tp", 0, 0, 3)
    got_max = got_max.reshape(tp_size, local_heads, 2, rows_here)
    got_tot = got_tot.reshape(tp_size, local_heads, 2, rows_here)
    got_sum = got_sum.reshape(tp_size, local_heads, 2, rows_here, VALUE_DIM)
    highest = jnp.max(got_max, axis=0)
    factor = jnp.exp(got_max - highest)
    totals_all = jnp.sum(factor * got_tot, axis=0)
    sums_all = jnp.sum(factor[..., None] * got_sum, axis=0)
    lambdas = lax.dynamic_slice_in_dim(diff_lambda, lax.axis_index("tp") * local_heads, local_heads)
    own_heads = head_norm(sums_all / totals_all[..., None], lambdas, head_gain)
    head_outputs = collect(own_heads, "tp", 0)
    out_grid = out_weight.reshape(HEADS, VALUE_DIM, out_weight.shape[1])
    projected = jnp.einsum(
        "hqe,hed->qd", head_outputs, out_grid, preferred_element_type=jnp.float32
    )
    after_mix = residual.astype(jnp.float32) + projected
    squares = over_copies(jnp.sum(after_mix * after_mix, axis=1), "tp")
    normed = (after_mix * lax.rsqrt(squares / D + epsilon)[:, None] * norm_gain).astype(
        jnp.bfloat16
    )
    full_rows = collect(normed, "tp", 1)
    hidden = jnp.dot(full_rows, up_whole, preferred_element_type=jnp.float32)
    activated = jnp.square(jax.nn.relu(hidden)).astype(jnp.bfloat16)
    partial_value = jnp.dot(activated, down_whole, preferred_element_type=jnp.float32)
    mixer_sum = sent_and_summed(partial_value, "tp", 1)
    return (after_mix + mixer_sum).astype(jnp.bfloat16)


def solution(mesh):
    return jax.shard_map(
        on_device,
        mesh=mesh,
        in_specs=(
            P("sp", "tp"),
            P("sp", "tp"),
            P(("sp", "tp"), None),
            P(("sp", "tp"), None),
            P(),
            P(),
            P(None, "tp"),
            P("tp"),
            P("sp", "tp"),
            P("tp", "sp"),
        ),
        out_specs=P("sp", "tp"),
        check_vma=False,
    )
```

profile of v0, /device:TPU:1, one launch (start us, length us, event | category | flops | bytes accessed | tf_op | source)
XLA Modules:
  0.0 231.3 jit_solution(17370695818168791017)
XLA Ops:
  6.5 0.0 copy-start
  6.5 0.0 all-gather.3.cloned.1.call-start
  6.5 1.4 pad_maximum_fusion.2
  8.0 0.0 all-gather.3.cloned.1.call-update
  8.0 0.0 all-gather.5.cloned.1.call-start
  8.1 1.5 pad_maximum_fusion.1
  9.6 0.0 all-gather.5.cloned.1.call-update
  9.6 1.0 copy.62
  10.6 0.9 broadcast_in_dim.10
  11.4 10.9 %all-to-all-start = ((bf16[8,128,256]{1,2,0:T(8,128)(2,1)}), bf16[8,128,256]{1,2,0:T(8,128)(2,1)}, u32[]{:S(2)}, u32[]{:S(2)}) async-start(bf16[8,128,256]{1,2,0:T(8,128)(2,1)} %broadcast_in_dim.10), calls=%async_computation | async-start | bytes 1048576 | tf_op jit(solution)/shard_map/all_to_all | solution.py:27
  22.3 72.8 %all-gather.3.cloned.1.call-done = bf16[1024,1024]{1,0:T(8,128)(2,1)} async-done(((bf16[16,1024]{1,0:T(8,128)(2,1)}), bf16[1024,1024]{1,0:T(8,128)(2,1)}) %all-gather.3.cloned.1.call-update) | async-done | bytes 2097168 | tf_op jit(solution)/shard_map/all_gather | solution.py:47
  95.1 1.7 fusion.34
  96.8 1.4 copy.93
  98.2 0.5 copy.92
  98.7 0.0 all-to-all-done
  98.7 2.3 %bitcast_reduce_fusion = (f32[2,4,2,128]{3,1,2,0:T(4,128)S(1)}, f32[2,2,1024,128,4]{3,2,4,1,0:T(8,128)S(1)}) fusion(bf16[1024,2,2,128,1]{0,3,4,2,1:T(8,128)(2,1)S(1)} %bitcast.73, bf16[128,2,4,2,128]{0,4,3,2,1:T(8,128)(2,1)} %bitcast.3), kind=kOutput, calls=%fused_computation.1 | convolution fusion | flops 541063168 | bytes 9969664 | tf_op jit(solution)/shard_map/qagcd,kacd->agcqk/dot_general | solution.py:117
  101.1 0.0 copy-start.1
  101.1 1.8 fusion.2
  102.9 0.0 copy-done.1
  102.9 3.2 %fusion.7 = f32[2,4,2,128,256]{4,3,2,1,0:T(8,128)} fusion(bf16[1024,2,256,1,1]{0,2,4,3,1:T(8,128)(2,1)S(1)} %bitcast.75, bf16[2,4,2,128,1024]{3,4,1,2,0:T(8,128)(2,1)S(1)} %get-tuple-element.8), kind=kOutput, calls=%fused_computation.9 | convolution fusion | flops 1073741824 | bytes 7340032 | tf_op jit(solution)/shard_map/agcqk,kae->agcqe/dot_general | solution.py:123
  106.0 2.8 %copy.72 = f32[8,2,128,256]{2,1,3,0:T(2,128)S(1)} copy(f32[8,2,128,256]{3,2,1,0:T(8,128)} %bitcast.74) | data formatting | bytes 4194304 | tf_op jit(solution)/shard_map/reshape | solution.py:132
  108.9 0.0 copy-start.5
  108.9 2.1 pad_maximum_fusion
  111.0 0.0 copy-start.3
  111.0 0.0 copy-start.2
  111.0 9.4 %all-to-all-start.1 = ((f32[8,2,128,258]{2,1,3,0:T(2,128)}), f32[8,2,128,258]{2,1,3,0:T(2,128)S(1)}, u32[]{:S(2)}, u32[]{:S(2)}) async-start(f32[8,2,128,258]{2,1,3,0:T(2,128)} %pad_maximum_fusion), calls=%async_computation.1 | async-start | bytes 4227072 | tf_op jit(solution)/shard_map/all_to_all | solution.py:54
  120.4 0.0 copy-start.4
  120.4 0.0 copy-done.5
  120.4 0.6 dynamic_slice.3
  121.0 25.8 %all-to-all-done.1 = f32[8,2,128,258]{2,1,3,0:T(2,128)S(1)} async-done(((f32[8,2,128,258]{2,1,3,0:T(2,128)}), f32[8,2,128,258]{2,1,3,0:T(2,128)S(1)}, u32[]{:S(2)}, u32[]{:S(2)}) %all-to-all-start.1) | async-done | bytes 2113568 | tf_op jit(solution)/shard_map/all_to_all | solution.py:54
  146.9 1.0 fusion.9
  147.8 0.1 bitcast_divide_fusion
  147.9 0.9 multiply_reduce_fusion.1
  148.9 0.0 copy-done.3
  148.9 0.1 multiply_convert_fusion.1
  149.0 0.1 copy.77
  149.2 12.8 %all_to_all.31 = bf16[8,1,128,256]{3,2,1,0:T(8,128)(2,1)S(1)} all-to-all(bf16[8,1,128,256]{3,2,1,0:T(8,128)(2,1)S(1)} %broadcast_in_dim.12), channel_id=1, replica_groups=mesh['sp'=64,'tp'=8] {'tp'}, dimensions={0} | all-to-all | bytes 1048576 | tf_op jit(solution)/shard_map/all_to_all | solution.py:27
  161.9 0.0 copy-done
  161.9 0.0 copy-done.2
  161.9 0.4 multiply_reduce_fusion
  162.3 8.0 %all_to_all.32 = f32[8,1,128]{2,1,0:T(1,128)S(1)} all-to-all(f32[8,1,128]{2,1,0:T(1,128)S(1)} %broadcast_in_dim.13), channel_id=1, replica_groups=mesh['sp'=64,'tp'=8] {'tp'}, dimensions={0} | all-to-all | bytes 8192 | tf_op jit(solution)/shard_map/all_to_all | solution.py:27
  170.4 0.0 copy-done.4
  170.4 0.1 multiply_convert_fusion
  170.5 0.1 copy.79
  170.6 0.1 broadcast_in_dim.28
  170.7 12.4 %all_to_all.33 = bf16[8,128,256]{1,2,0:T(8,128)(2,1)S(1)} all-to-all(bf16[8,128,256]{1,2,0:T(8,128)(2,1)S(1)} %broadcast_in_dim.28), channel_id=1, replica_groups=mesh['sp'=64,'tp'=8] {'tp'}, dimensions={0} | all-to-all | bytes 1048576 | tf_op jit(solution)/shard_map/all_to_all | solution.py:27
  183.1 15.0 %all-gather.5.cloned.1.call-done = bf16[2048,2048]{1,0:T(8,128)(2,1)} async-done(((bf16[32,2048]{1,0:T(8,128)(2,1)}), bf16[2048,2048]{1,0:T(8,128)(2,1)}) %all-gather.5.cloned.1.call-update) | async-done | bytes 8388624 | tf_op jit(solution)/shard_map/all_gather | solution.py:17
  198.1 5.6 %fusion.3 = f32[128,2048]{1,0:T(8,128)S(1)} fusion(bf16[2048,2048]{1,0:T(8,128)(2,1)} %all-gather.5.cloned.1.call-done, bf16[128,2048]{0,1:T(8,128)(2,1)S(1)} %bitcast.78), kind=kOutput, calls=%fused_computation.5 | convolution fusion | flops 1074135040 | bytes 9961472 | tf_op jit(solution)/shard_map/dot_general | solution.py:158
  203.7 0.1 copy.112
  203.8 19.9 %all_to_all.34 = f32[8,128,256]{2,1,0:T(8,128)S(1)} all-to-all(f32[8,128,256]{2,1,0:T(8,128)S(1)} %bitcast.72), channel_id=1, replica_groups=mesh['sp'=64,'tp'=8] {'tp'}, dimensions={0} | all-to-all | bytes 2097152 | tf_op jit(solution)/shard_map/all_to_all | solution.py:78
  223.7 0.1 reduce_sum.72
  223.8 0.6 add_convert_fusion
  (14 shorter events, 0.2 us)
Async XLA Ops:
  6.5 155.4 %copy-start = (bf16[2048,256]{1,0:T(8,128)(2,1)S(1)}, bf16[2048,256]{1,0:T(8,128)(2,1)}, u32[]{:S(2)}) copy-start(bf16[2048,256]{1,0:T(8,128)(2,1)} %param.16) | copy-start | bytes 3145732
  6.5 88.5 %all-gather.3.cloned.1.call-start = ((), (), s32[]{:S(2)}) async-start(), calls=%async_computation.6 | async-start | bytes 2129920 | tf_op jit(solution)/shard_map/all_gather | solution.py:47
  8.0 190.1 %all-gather.5.cloned.1.call-start = ((), (), s32[]{:S(2)}) async-start(), calls=%async_computation.7 | async-start | bytes 8519680 | tf_op jit(solution)/shard_map/all_gather | solution.py:17
  11.4 87.2 %all-to-all-start = ((bf16[8,128,256]{1,2,0:T(8,128)(2,1)}), bf16[8,128,256]{1,2,0:T(8,128)(2,1)}, u32[]{:S(2)}, u32[]{:S(2)}) async-start(bf16[8,128,256]{1,2,0:T(8,128)(2,1)} %broadcast_in_dim.10), calls=%async_computation | async-start | bytes 1048576 | tf_op jit(solution)/shard_map/all_to_all | solution.py:27
  101.1 1.8 copy-start.1
  108.9 11.5 %copy-start.5 = (f32[8]{0:T(128)S(1)}, f32[8]{0:T(128)}, u32[]{:S(2)}) copy-start(f32[8]{0:T(128)} %param.14) | copy-start | bytes 100
  111.0 37.9 %copy-start.3 = (f32[256]{0:T(256)S(1)}, f32[256]{0:T(256)}, u32[]{:S(2)}) copy-start(f32[256]{0:T(256)} %param.15) | copy-start | bytes 3076
  111.0 50.9 %copy-start.2 = (bf16[128,256]{1,0:T(8,128)(2,1)S(1)}, bf16[128,256]{1,0:T(8,128)(2,1)}, u32[]{:S(2)}) copy-start(bf16[128,256]{1,0:T(8,128)(2,1)} %param.10) | copy-start | bytes 196612
  111.0 35.8 %all-to-all-start.1 = ((f32[8,2,128,258]{2,1,3,0:T(2,128)}), f32[8,2,128,258]{2,1,3,0:T(2,128)S(1)}, u32[]{:S(2)}, u32[]{:S(2)}) async-start(f32[8,2,128,258]{2,1,3,0:T(2,128)} %pad_maximum_fusion), calls=%async_computation.1 | async-start | bytes 4227072 | tf_op jit(solution)/shard_map/all_to_all | solution.py:54
  120.4 50.0 %copy-start.4 = (f32[256]{0:T(256)S(1)}, f32[256]{0:T(256)}, u32[]{:S(2)}) copy-start(f32[256]{0:T(256)} %param.17) | copy-start | bytes 3076
Sparse Core Ops, SparseCore 0:
  10.4 84.6 all-gather.2
  98.1 99.9 all-gather.4
where the time goes:
time: 232 us; the launch traced here: 231 us
  waiting for transfers between devices  114 us (49%)
  blocking collectives  53.1 us (23%)
  starting transfers between devices  20.3 us (9%)
  between operations  13.6 us (6%)
  matrix products  11.5 us (5%)
  other arithmetic  9.83 us (4%)
  local copies, waits for them, and re-layouts  9.31 us (4%)
    all_gather x1, waiting for transfers between devices, sent_together(): lax.all_gather(both, axis, axis=dim, tiled=True)  72.8 us
    all_to_all x3, blocking collectives, from_everyone(): return lax.all_to_all(copies, axis, split_axis=0, concat_axis=0, tiled=True)  33.2 us
    all_to_all x1, waiting for transfers between devices, side_by_side(): lax.all_to_all(both, axis, split_axis=split_dim, concat_axis=concat_dim,...  25.8 us
    all_to_all x1, blocking collectives, sent_and_summed(): lax.all_to_all(parts, axis, split_axis=0, concat_axis=0, tiled=True)  19.9 us
    all_gather x1, waiting for transfers between devices, turned_gather(): lax.all_gather(both, axis, axis=0, tiled=True)  15 us
    all_to_all x1, starting transfers between devices, from_everyone(): return lax.all_to_all(copies, axis, split_axis=0, concat_axis=0, tiled=True)  10.9 us
    all_to_all x1, starting transfers between devices, side_by_side(): lax.all_to_all(both, axis, split_axis=split_dim, concat_axis=concat_dim,...  9.39 us
    dot_general x1, matrix products, on_device(): jnp.dot(activated, down_whole, preferred_element_type=jnp.float32)  5.59 us
  transfers between devices with their start and end apart: 4, of which 3 were waited for; matrix products, arithmetic and copies ran while one was open for 10% of the time, Pallas kernels for 0%

commit v1 on v0

--- a/solution.py
+++ b/solution.py
@@ -14,7 +14,13 @@
 def turned_gather(arrays, axis, dims):
     turned = [jnp.moveaxis(a, dim, 0) for a, dim in zip(arrays, dims)]
     both = jnp.concatenate([t.reshape(len(t), -1) for t in turned], axis=1)
-    whole, at, finished = (lax.all_gather(both, axis, axis=0, tiled=True), 0, [])
+    whole, at, finished = (
+        jnp.concatenate(
+            jax.lax.all_to_all(jnp.stack(jax.lax.axis_size(axis) * [both], axis=0), axis, 0, 0), 0
+        ),
+        0,
+        [],
+    )
     for t, dim in zip(turned, dims):
         share = whole[:, at : at + t[0].size].reshape(-1, *t.shape[1:])
         finished.append(jnp.moveaxis(share, 0, dim))

time: 232 us -> 427 us (1.84)
  the two profiles are of different devices: /device:TPU:1 before, /device:TPU:24 now
where the time goes in v1:
time: 427 us
  blocking collectives  249 us (58%)
  waiting for transfers between devices  121 us (28%)
  between operations  13.7 us (3%)
  starting transfers between devices  12.2 us (3%)
  matrix products  11.4 us (3%)
  local copies, waits for them, and re-layouts  11.1 us (3%)
  other arithmetic  8.35 us (2%)
    all_to_all x1, blocking collectives, turned_gather(): jax.lax.all_to_all(jnp.stack(jax.lax.axis_size(axis) * [both], axis=0), a...  210 us
    all_gather x1, waiting for transfers between devices, sent_together(): lax.all_gather(both, axis, axis=dim, tiled=True)  83.9 us
    all_to_all x1, waiting for transfers between devices, side_by_side(): lax.all_to_all(both, axis, split_axis=split_dim, concat_axis=concat_dim,...  26.7 us
    all_to_all x2, blocking collectives, from_everyone(): return lax.all_to_all(copies, axis, split_axis=0, concat_axis=0, tiled=True)  20.4 us
    all_to_all x1, blocking collectives, sent_and_summed(): lax.all_to_all(parts, axis, split_axis=0, concat_axis=0, tiled=True)  18.4 us
    all_to_all x2, waiting for transfers between devices, from_everyone(): return lax.all_to_all(copies, axis, split_axis=0, concat_axis=0, tiled=True)  10.2 us
  transfers between devices with their start and end apart: 4, of which 3 were waited for; matrix products, arithmetic and copies ran while one was open for 1% of the time, Pallas kernels for 0%

profile of v1, /device:TPU:24, one launch (start us, length us, event | category | flops | bytes accessed | tf_op | source)
XLA Modules:
  0.0 426.6 jit_solution(12663066150266105149)
XLA Ops:
  6.5 0.0 copy-start
  6.5 0.0 all-gather.2.cloned.1.call-start
  6.5 1.4 pad_maximum_fusion.2
  8.0 0.0 all-gather.2.cloned.1.call-update
  8.0 1.0 copy.62
  9.0 0.9 broadcast_in_dim.10
  9.8 4.3 %all-to-all-start = ((bf16[8,128,256]{1,2,0:T(8,128)(2,1)}), bf16[8,128,256]{1,2,0:T(8,128)(2,1)}, u32[]{:S(2)}, u32[]{:S(2)}) async-start(bf16[8,128,256]{1,2,0:T(8,128)(2,1)} %broadcast_in_dim.10), calls=%async_computation | async-start | bytes 1048576 | tf_op jit(solution)/shard_map/all_to_all | solution.py:33
  14.1 83.9 %all-gather.2.cloned.1.call-done = bf16[1024,1024]{1,0:T(8,128)(2,1)} async-done(((bf16[16,1024]{1,0:T(8,128)(2,1)}), bf16[1024,1024]{1,0:T(8,128)(2,1)}) %all-gather.2.cloned.1.call-update) | async-done | bytes 2097168 | tf_op jit(solution)/shard_map/all_gather | solution.py:53
  98.1 1.7 fusion.34
  99.8 1.3 copy.93
  101.1 0.5 copy.92
  101.6 0.0 all-to-all-done
  101.6 2.3 bitcast_reduce_fusion
  104.0 0.0 copy-start.1
  104.0 1.8 fusion.2
  105.8 0.0 copy-done.1
  105.8 3.1 fusion.7
  108.9 2.8 copy.72
  111.8 0.0 copy-start.7
  111.8 2.2 pad_maximum_fusion
  114.0 0.0 copy-start.5
  114.0 0.0 copy-start.4
  114.0 4.4 %all-to-all-start.1 = ((f32[8,2,128,258]{2,1,3,0:T(2,128)}), f32[8,2,128,258]{2,1,3,0:T(2,128)S(1)}, u32[]{:S(2)}, u32[]{:S(2)}) async-start(f32[8,2,128,258]{2,1,3,0:T(2,128)} %pad_maximum_fusion), calls=%async_computation.1 | async-start | bytes 4227072 | tf_op jit(solution)/shard_map/all_to_all | solution.py:60
  118.4 0.0 copy-start.6
  118.4 0.0 copy-done.7
  118.4 0.6 dynamic_slice.3
  119.0 26.7 %all-to-all-done.1 = f32[8,2,128,258]{2,1,3,0:T(2,128)S(1)} async-done(((f32[8,2,128,258]{2,1,3,0:T(2,128)}), f32[8,2,128,258]{2,1,3,0:T(2,128)S(1)}, u32[]{:S(2)}, u32[]{:S(2)}) %all-to-all-start.1) | async-done | bytes 2113568 | tf_op jit(solution)/shard_map/all_to_all | solution.py:60
  145.8 0.0 copy-start.2
  145.8 0.0 copy-start.3
  145.8 1.0 fusion.9
  146.8 0.1 bitcast_divide_fusion
  146.9 0.9 multiply_reduce_fusion.1
  147.8 0.0 copy-done.5
  147.8 0.1 multiply_convert_fusion.1
  147.9 0.1 copy.77
  148.1 12.8 %all_to_all.36 = bf16[8,1,128,256]{3,2,1,0:T(8,128)(2,1)S(1)} all-to-all(bf16[8,1,128,256]{3,2,1,0:T(8,128)(2,1)S(1)} %broadcast_in_dim.12), channel_id=1, replica_groups=mesh['sp'=64,'tp'=8] {'tp'}, dimensions={0} | all-to-all | bytes 1048576 | tf_op jit(solution)/shard_map/all_to_all | solution.py:33
  160.8 0.0 copy-done
  160.8 0.0 copy-done.4
  160.8 0.4 multiply_reduce_fusion
  161.3 7.7 %all_to_all.37 = f32[8,1,128]{2,1,0:T(1,128)S(1)} all-to-all(f32[8,1,128]{2,1,0:T(1,128)S(1)} %broadcast_in_dim.13), channel_id=1, replica_groups=mesh['sp'=64,'tp'=8] {'tp'}, dimensions={0} | all-to-all | bytes 8192 | tf_op jit(solution)/shard_map/all_to_all | solution.py:33
  168.9 0.0 copy-done.6
  168.9 0.1 multiply_convert_fusion
  169.0 0.1 copy.79
  169.1 0.9 broadcast_in_dim.28
  170.0 3.5 all-to-all-start.4
  173.5 0.0 copy-done.2
  173.5 0.0 copy-done.3
  173.6 10.2 %all-to-all-done.4 = bf16[8,128,256]{1,2,0:T(8,128)(2,1)S(1)} async-done(((bf16[8,128,256]{1,2,0:T(8,128)(2,1)}), bf16[8,128,256]{1,2,0:T(8,128)(2,1)S(1)}, u32[]{:S(2)}, u32[]{:S(2)}) %all-to-all-start.4) | async-done | bytes 524320 | tf_op jit(solution)/shard_map/all_to_all | solution.py:33
  183.8 1.1 stack.2
  184.8 210.2 %all_to_all.38 = bf16[64,32,2048]{2,1,0:T(8,128)(2,1)} all-to-all(bf16[64,32,2048]{2,1,0:T(8,128)(2,1)S(1)} %stack.2), channel_id=1, replica_groups=mesh['sp'=64,'tp'=8] {'sp'}, dimensions={0} | all-to-all | bytes 16777216 | tf_op jit(solution)/shard_map/all_to_all | solution.py:19
  395.0 5.6 %fusion.3 = f32[128,2048]{1,0:T(8,128)S(1)} fusion(bf16[2048,2048]{1,0:T(8,128)(2,1)} %bitcast.73, bf16[128,2048]{0,1:T(8,128)(2,1)S(1)} %bitcast.80), kind=kOutput, calls=%fused_computation.5 | convolution fusion | flops 1074135040 | bytes 9961472 | tf_op jit(solution)/shard_map/dot_general | solution.py:164
  400.6 0.1 copy.112
  400.7 18.4 %all_to_all.39 = f32[8,128,256]{2,1,0:T(8,128)S(1)} all-to-all(f32[8,128,256]{2,1,0:T(8,128)S(1)} %bitcast.74), channel_id=1, replica_groups=mesh['sp'=64,'tp'=8] {'tp'}, dimensions={0} | all-to-all | bytes 2097152 | tf_op jit(solution)/shard_map/all_to_all | solution.py:84
  419.1 0.1 reduce_sum.72
  419.1 0.6 add_convert_fusion
  (15 shorter events, 0.2 us)
Async XLA Ops:
  6.5 154.3 %copy-start = (bf16[2048,256]{1,0:T(8,128)(2,1)S(1)}, bf16[2048,256]{1,0:T(8,128)(2,1)}, u32[]{:S(2)}) copy-start(bf16[2048,256]{1,0:T(8,128)(2,1)} %param.16) | copy-start | bytes 3145732
  6.5 91.6 %all-gather.2.cloned.1.call-start = ((), (), s32[]{:S(2)}) async-start(), calls=%async_computation.7 | async-start | bytes 2129920 | tf_op jit(solution)/shard_map/all_gather | solution.py:53
  9.8 91.8 %all-to-all-start = ((bf16[8,128,256]{1,2,0:T(8,128)(2,1)}), bf16[8,128,256]{1,2,0:T(8,128)(2,1)}, u32[]{:S(2)}, u32[]{:S(2)}) async-start(bf16[8,128,256]{1,2,0:T(8,128)(2,1)} %broadcast_in_dim.10), calls=%async_computation | async-start | bytes 1048576 | tf_op jit(solution)/shard_map/all_to_all | solution.py:33
  104.0 1.8 copy-start.1
  111.8 6.6 %copy-start.7 = (f32[8]{0:T(128)S(1)}, f32[8]{0:T(128)}, u32[]{:S(2)}) copy-start(f32[8]{0:T(128)} %param.14) | copy-start | bytes 100
  114.0 33.8 %copy-start.5 = (f32[256]{0:T(256)S(1)}, f32[256]{0:T(256)}, u32[]{:S(2)}) copy-start(f32[256]{0:T(256)} %param.15) | copy-start | bytes 3076
  114.0 46.9 %copy-start.4 = (bf16[128,256]{1,0:T(8,128)(2,1)S(1)}, bf16[128,256]{1,0:T(8,128)(2,1)}, u32[]{:S(2)}) copy-start(bf16[128,256]{1,0:T(8,128)(2,1)} %param.10) | copy-start | bytes 196612
  114.0 31.7 %all-to-all-start.1 = ((f32[8,2,128,258]{2,1,3,0:T(2,128)}), f32[8,2,128,258]{2,1,3,0:T(2,128)S(1)}, u32[]{:S(2)}, u32[]{:S(2)}) async-start(f32[8,2,128,258]{2,1,3,0:T(2,128)} %pad_maximum_fusion), calls=%async_computation.1 | async-start | bytes 4227072 | tf_op jit(solution)/shard_map/all_to_all | solution.py:60
  118.4 50.6 %copy-start.6 = (f32[256]{0:T(256)S(1)}, f32[256]{0:T(256)}, u32[]{:S(2)}) copy-start(f32[256]{0:T(256)} %param.17) | copy-start | bytes 3076
  145.8 27.7 %copy-start.2 = (bf16[1024,32]{0,1:T(8,128)(2,1)S(1)}, bf16[1024,32]{0,1:T(8,128)(2,1)}, u32[]{:S(2)}) copy-start(bf16[1024,32]{0,1:T(8,128)(2,1)} %param.19) | copy-start | bytes 196612
  145.8 27.7 %copy-start.3 = (bf16[32,1024]{1,0:T(8,128)(2,1)S(1)}, bf16[32,1024]{1,0:T(8,128)(2,1)}, u32[]{:S(2)}) copy-start(bf16[32,1024]{1,0:T(8,128)(2,1)} %param.18) | copy-start | bytes 196612
  170.0 13.7 %all-to-all-start.4 = ((bf16[8,128,256]{1,2,0:T(8,128)(2,1)}), bf16[8,128,256]{1,2,0:T(8,128)(2,1)S(1)}, u32[]{:S(2)}, u32[]{:S(2)}) async-start(bf16[8,128,256]{1,2,0:T(8,128)(2,1)} %broadcast_in_dim.28), calls=%async_computation.4 | async-start | bytes 1048576 | tf_op jit(solution)/shard_map/all_to_all | solution.py:33
Sparse Core Ops, SparseCore 0:
  10.4 87.6 all-gather.1
